TPU v7x, 512 devices: a whole 4x8x8 slice. The times are simulated.
512 devices in a mesh: sp: 128 (over z, y, core), tp: 4 (over x).
Axes of the slice: x: 4, y: 8, z: 8, core: 2. Of those that a mesh axis runs over, the one named last changes fastest.
Arguments:
- tokens: bfloat16 [32768, 2048], P(('sp', 'tp')), may hold values from -16 to 16
- w_query: bfloat16 [2048, 1024], P(None, 'tp'), may hold values from -1 to 1
- w_key: bfloat16 [2048, 256], P(None, 'tp'), may hold values from -1 to 1
- w_value: bfloat16 [2048, 256], P(None, 'tp'), may hold values from -0.125 to 0.125
- w_gate: bfloat16 [2048, 16], P(None, 'tp'), may hold values from -0.125 to 0.125
- gate_bias: float32 [16], P('tp'), as said below
- w_output: bfloat16 [1024, 2048], P('tp'), may hold values from -0.1875 to 0.1875
Outputs:
- mixed: bfloat16 [32768, 2048], P(('sp', 'tp'))
Inputs may be any that keep to these rules, and one draw needn't show every extreme that they name: `gate_bias`: each head's forget gate bias is 4 or more; there is no upper bound.
All inputs are finite; a program needn't handle non-finite values.
Results may differ from a plain program's by a relative error of at most 0.012.
The roundings to bfloat16 on the way count: a program that leaves them out, or rounds other values in their place, can miss the bound.
Values may be sent and summed in bfloat16 or wider, within the bound.
No kernel may reach another device: no remote copies, remote signals or barrier semaphores. Data moves between devices by JAX's collectives and lax.ppermute only.
A program may use at most 64 MiB of HBM per device.

v0:
```python
import math
import jax
import jax.numpy as jnp
from jax import lax
from jax.sharding import Mesh
from jax.sharding import PartitionSpec as P

HEAD = 64
SP = ("sp_0", "sp_1", "sp_2")
SP_TP = ("sp_0", "sp_1", "sp_2", "tp")
masked_value = -1e30


def copy_for_each(value, axis):
    copies = jnp.broadcast_to(value, (lax.axis_size(axis), *value.shape))
    return lax.all_to_all(copies, axis, split_axis=0, concat_axis=0, tiled=True)


def in_order(pieces, dim):
    lengths = list(pieces.shape[1:])
    lengths[dim] *= pieces.shape[0]
    return jnp.moveaxis(pieces, 0, dim).reshape(lengths)


def collect(value, axis, dim):
    pieces = copy_for_each(value, axis)
    return in_order(pieces, dim)


def all_blocks(value, axes, sequence):
    pieces = value
    for k in sequence:
        pieces = lax.all_gather(pieces, axes[k])
    done = sequence[::-1]
    back = [done.index(k) for k in range(len(axes))]
    pieces = pieces.transpose(*back, *range(len(axes), pieces.ndim))
    return pieces.reshape(-1, *value.shape)


def whole_of(value, axes, sequence, dim):
    return in_order(all_blocks(value, axes, sequence), dim)


def in_blocks(value, dim, count):
    lengths = value.shape
    pieces = value.reshape(*lengths[:dim], count, lengths[dim] // count, *lengths[dim + 1 :])
    return jnp.moveaxis(pieces, dim, 0)


def sum_at_owner(value, axis, dim):
    pieces = in_blocks(value, dim, lax.axis_size(axis))
    arrived = lax.all_to_all(pieces, axis, split_axis=0, concat_axis=0, tiled=True)
    return arrived.astype(jnp.float32).sum(axis=0)


def softmax_update(
    carry_state,
    query_here,
    query_cumul,
    query_position,
    key_here,
    value_here,
    key_cumul,
    key_position,
):
    row_peak, row_mass, row_accum = carry_state
    scores = jnp.einsum(
        "kgtd,skd->kgts", query_here, key_here, preferred_element_type=jnp.float32
    ) * HEAD ** (-0.5)
    scores = scores + query_cumul[:, :, :, None] - key_cumul[:, :, None, :]
    allowed = key_position[None, :] <= query_position[:, None]
    scores = jnp.where(allowed, scores, masked_value)
    new_peak = jnp.maximum(row_peak, jnp.max(scores, axis=3))
    weights = jnp.where(allowed, jnp.exp(scores - new_peak[:, :, :, None]), 0.0)
    rescale = jnp.exp(row_peak - new_peak)
    row_mass = row_mass * rescale + jnp.sum(weights, axis=3)
    row_accum = row_accum * rescale[:, :, :, None] + jnp.einsum(
        "kgts,skd->kgtd",
        weights.astype(jnp.bfloat16),
        value_here,
        preferred_element_type=jnp.float32,
    )
    return (new_peak, row_mass, row_accum)


def shards(tokens, w_query, w_key, w_value, w_gate, gate_bias, w_output):
    sp_count = lax.axis_size(SP)
    sp_rank = lax.axis_index(SP)
    query_cols = w_query.shape[1]
    key_cols = w_key.shape[1]
    heads_here = w_gate.shape[1]
    kv_heads_here = key_cols // HEAD
    group_size = heads_here // kv_heads_here
    joined = jnp.concatenate([w_query, w_key, w_value, w_gate], axis=1)
    projected = jnp.dot(
        collect(tokens, "tp", 0), joined, preferred_element_type=jnp.float32
    ).astype(jnp.bfloat16)
    local_rows = projected.shape[0]
    half_rows = local_rows // 2
    second_block = 2 * sp_rank + 1
    own_gates = jax.nn.log_sigmoid(
        projected[:, query_cols + 2 * key_cols :].astype(jnp.float32) + gate_bias
    )
    totals = jnp.sum(own_gates.reshape(2, half_rows, heads_here), axis=1)
    all_totals = whole_of(totals[None], (("sp_0", "sp_1"), "sp_2"), (0, 1), 0)
    ordered = all_totals.reshape(2 * sp_count, heads_here)
    prefix_sums = jnp.cumsum(ordered, axis=0) - ordered
    queries = (
        projected[:, :query_cols]
        .reshape(2, half_rows, kv_heads_here, group_size, HEAD)
        .transpose(0, 2, 3, 1, 4)
    )
    query_blocks = (2 * sp_rank, second_block)
    query_cumul = []
    query_position = []
    for side_index in range(2):
        base_value = lax.dynamic_index_in_dim(
            prefix_sums, query_blocks[side_index], 0, keepdims=False
        )
        cumul_rows = base_value[None, :] + jnp.cumsum(
            own_gates[side_index * half_rows : (side_index + 1) * half_rows], axis=0
        )
        query_cumul.append(
            cumul_rows.reshape(half_rows, kv_heads_here, group_size).transpose(1, 2, 0)
        )
        query_position.append(
            query_blocks[side_index] * half_rows + jnp.arange(half_rows, dtype=jnp.int32)
        )
    initial = (
        jnp.full((2, kv_heads_here, group_size, half_rows), masked_value, jnp.float32),
        jnp.zeros((2, kv_heads_here, group_size, half_rows), jnp.float32),
        jnp.zeros((2, kv_heads_here, group_size, half_rows, HEAD), jnp.float32),
    )
    gathered = lax.all_gather(projected[:, query_cols:], SP, axis=0, tiled=True)
    row_count = gathered.shape[0]
    piece_blocks = row_count // half_rows
    per_step = math.gcd(piece_blocks, max(1, 1024 // half_rows))
    step_rows = per_step * half_rows
    step_count = row_count // step_rows
    first_row = half_rows * jnp.arange(piece_blocks, dtype=jnp.int32)
    owner_rank = first_row // local_rows
    half_index = first_row % local_rows // half_rows
    block_ids = 2 * owner_rank + half_index
    gate_logs = jax.nn.log_sigmoid(gathered[:, 2 * key_cols :].astype(jnp.float32) + gate_bias)
    gate_logs = gate_logs.reshape(piece_blocks, half_rows, heads_here)
    base_values = jnp.take(prefix_sums, block_ids, axis=0)
    key_cumul_all = (base_values[:, None, :] + jnp.cumsum(gate_logs, axis=1)).reshape(
        row_count, kv_heads_here, group_size
    )
    key_position_all = (
        block_ids[:, None] * half_rows + jnp.arange(half_rows, dtype=jnp.int32)[None, :]
    ).reshape(row_count)
    earliest = jnp.min(block_ids.reshape(step_count, per_step), axis=1)

    def one_step(step_index, inner_state):
        start_row = step_index * step_rows
        block_rows = lax.dynamic_slice_in_dim(gathered, start_row, step_rows, 0)
        key_here = block_rows[:, :key_cols].reshape(step_rows, kv_heads_here, HEAD)
        value_here = block_rows[:, key_cols : 2 * key_cols].reshape(step_rows, kv_heads_here, HEAD)
        key_cumul = lax.dynamic_slice_in_dim(key_cumul_all, start_row, step_rows, 0).transpose(
            1, 2, 0
        )
        key_position = lax.dynamic_slice_in_dim(key_position_all, start_row, step_rows, 0)
        first_id = earliest[step_index]
        results = []
        for side_index in range(2):
            head_state = tuple((member[side_index] for member in inner_state))

            def compute(head_state, side_index=side_index):
                return softmax_update(
                    head_state,
                    queries[side_index],
                    query_cumul[side_index],
                    query_position[side_index],
                    key_here,
                    value_here,
                    key_cumul,
                    key_position,
                )

            head_state = lax.cond(
                first_id <= query_blocks[side_index],
                compute,
                lambda unchanged: unchanged,
                head_state,
            )
            results.append(head_state)
        return tuple((jnp.stack([results[0][member], results[1][member]]) for member in range(3)))

    row_peak, row_mass, row_accum = lax.fori_loop(0, step_count, one_step, initial)
    attended = (row_accum / row_mass[:, :, :, :, None]).astype(jnp.bfloat16)
    attended = attended.transpose(0, 3, 1, 2, 4).reshape(local_rows, heads_here * HEAD)
    mixed = sum_at_owner(
        jnp.dot(attended, w_output, preferred_element_type=jnp.float32).astype(jnp.bfloat16),
        "tp",
        0,
    )
    return mixed.astype(jnp.bfloat16)


def solution(mesh):
    finer = Mesh(mesh.devices.reshape(8, 8, 2, mesh.shape["tp"]), ("sp_0", "sp_1", "sp_2", "tp"))
    placed = (
        P(SP_TP, None),
        P(None, "tp"),
        P(None, "tp"),
        P(None, "tp"),
        P(None, "tp"),
        P("tp"),
        P("tp", None),
    )
    return jax.shard_map(
        shards, mesh=finer, in_specs=placed, out_specs=P(SP_TP, None), check_vma=False
    )
```

profile of v0, /device:TPU:504, one launch (start us, length us, event | category | flops | bytes accessed | tf_op | source)
XLA Modules:
  0.0 388.9 jit_solution(7107253783128811441)
XLA Ops:
  8.7 4.3 %all-to-all-start = ((bf16[4,64,2048]{2,1,0:T(8,128)(2,1)}), bf16[4,64,2048]{2,1,0:T(8,128)(2,1)S(1)}, u32[]{:S(2)}, u32[]{:S(2)}) async-start(bf16[4,64,2048]{2,1,0:T(8,128)(2,1)} %broadcast_in_dim.67), calls=%async_computation | async-start | bytes 2097152 | tf_op jit(solution)/shard_map/all_to_all | solution.py:16
  14.7 13.4 %all-to-all-done = bf16[4,64,2048]{2,1,0:T(8,128)(2,1)S(1)} async-done(((bf16[4,64,2048]{2,1,0:T(8,128)(2,1)}), bf16[4,64,2048]{2,1,0:T(8,128)(2,1)S(1)}, u32[]{:S(2)}, u32[]{:S(2)}) %all-to-all-start) | async-done | bytes 1048608 | tf_op jit(solution)/shard_map/all_to_all | solution.py:16
  28.1 2.5 fusion.47
  31.9 47.2 %all-gather.2 = f32[64,2,4]{2,1,0:T(2,128)S(1)} all-gather(f32[1,2,4]{2,1,0:T(2,128)S(1)} %bitcast.213), channel_id=2, replica_groups=mesh['sp_0'=8,'sp_1'=8,'sp_2'=2,'tp'=4] {'sp_0','sp_1'}, dimensions={0}, use_global_device_ids=true | all-gather | bytes 2080 | tf_op jit(solution)/shard_map/all_gather | solution.py:33
  84.7 35.0 %all-gather.5.cloned.1.call-done = bf16[32768,132]{0,1:T(8,128)(2,1)} async-done(((bf16[256,132]{0,1:T(8,128)(2,1)}), bf16[32768,132]{0,1:T(8,128)(2,1)}) %all-gather.5.cloned.1.call-update) | async-done | bytes 8650768 | tf_op jit(solution)/shard_map/all_gather | solution.py:134
  122.7 238.2 %while.18 = (s32[]{:T(128)}, f32[2,1,4,128]{3,2,1,0:T(4,128)S(1)}, f32[2,1,4,128]{3,2,1,0:T(4,128)S(1)}, f32[2,1,4,128,64]{3,4,2,1,0:T(8,128)S(1)}, s32[32]{0:T(...) while((s32[]{:T(128)}, f32[2,1,4,128]{3,2,1,0:T(4,128)S(1)}, ...), condition=%wide.region_16.17_spmd.clone, body=%wide.region_7.16_spmd.clone.sunk | while | flops 280433920 | bytes 16568903 | solution.py:190
  127.9 2.2 conditional.7
  135.4 2.2 conditional.7
  142.8 2.2 conditional.7
  150.2 2.2 conditional.7
  157.7 2.2 conditional.7
  165.1 2.2 conditional.7
  172.6 2.2 conditional.7
  180.0 2.2 conditional.7
  187.5 2.2 conditional.7
  194.9 2.2 conditional.7
  202.4 2.2 conditional.7
  209.8 2.2 conditional.7
  217.2 2.2 conditional.7
  224.7 2.2 conditional.7
  232.1 2.2 conditional.7
  239.6 2.2 conditional.7
  247.0 2.2 conditional.7
  254.5 2.2 conditional.7
  261.9 2.2 conditional.7
  276.8 2.2 conditional.7
  291.7 2.2 conditional.7
  306.6 2.2 conditional.7
  321.5 2.2 conditional.7
  336.4 2.2 conditional.7
  351.2 2.2 conditional.7
  361.6 19.5 %all_to_all.10 = bf16[4,64,2048]{2,1,0:T(8,128)(2,1)S(1)} all-to-all(bf16[4,64,2048]{2,1,0:T(8,128)(2,1)S(1)} %bitcast.197), channel_id=1, replica_groups=mesh['sp_0'=8,'sp_1'=8,'sp_2'=2,'tp'=4] {'tp'}, dimensions={0} | all-to-all | bytes 2097152 | tf_op jit(solution)/shard_map/all_to_all | solution.py:52
  (907 shorter events, 290.7 us)
Async XLA Ops:
  6.5 354.6 %copy-start = (bf16[256,2048]{1,0:T(8,128)(2,1)S(1)}, bf16[256,2048]{1,0:T(8,128)(2,1)}, u32[]{:S(2)}) copy-start(bf16[256,2048]{1,0:T(8,128)(2,1)} %param.19) | copy-start | bytes 3145732
  6.5 6.5 %copy-start.3 = (bf16[2048,4]{0,1:T(4,128)(2,1)S(1)}, bf16[2048,4]{0,1:T(4,128)(2,1)}, u32[]{:S(2)}) copy-start(bf16[2048,4]{0,1:T(4,128)(2,1)} %param.17) | copy-start | bytes 49156
  6.5 7.6 %copy-start.1 = (bf16[2048,64]{0,1:T(8,128)(2,1)S(1)}, bf16[2048,64]{0,1:T(8,128)(2,1)}, u32[]{:S(2)}) copy-start(bf16[2048,64]{0,1:T(8,128)(2,1)} %param.16) | copy-start | bytes 786436
  6.5 7.8 %copy-start.2 = (bf16[2048,64]{0,1:T(8,128)(2,1)S(1)}, bf16[2048,64]{0,1:T(8,128)(2,1)}, u32[]{:S(2)}) copy-start(bf16[2048,64]{0,1:T(8,128)(2,1)} %param.15) | copy-start | bytes 786436
  8.7 19.4 %all-to-all-start = ((bf16[4,64,2048]{2,1,0:T(8,128)(2,1)}), bf16[4,64,2048]{2,1,0:T(8,128)(2,1)S(1)}, u32[]{:S(2)}, u32[]{:S(2)}) async-start(bf16[4,64,2048]{2,1,0:T(8,128)(2,1)} %broadcast_in_dim.67), calls=%async_computation | async-start | bytes 2097152 | tf_op jit(solution)/shard_map/all_to_all | solution.py:16
  13.0 106.7 %all-gather.5.cloned.1.call-start = ((), (), s32[]{:S(2)}) async-start(), calls=%async_computation.2 | async-start | bytes 8982528 | tf_op jit(solution)/shard_map/all_gather | solution.py:134
  28.1 3.5 copy-start.4
Sparse Core Ops, SparseCore 0:
  31.4 88.1 all-gather.4
where the time goes:
time: 390 us; the launch traced here: 389 us
  matrix products  91.4 us (23%)
  blocking collectives  68.7 us (18%)
  local copies, waits for them, and re-layouts  59.3 us (15%)
  other arithmetic  55.4 us (14%)
  waiting for transfers between devices  48.4 us (12%)
  loops' own time  47.7 us (12%)
  between operations  13.7 us (4%)
  starting transfers between devices  4.29 us (1%)
    all_gather x2, blocking collectives, all_blocks(): pieces = lax.all_gather(pieces, axes[k])  49.1 us
    dot_general x64, matrix products, softmax_update(): jnp.einsum('kgtd,skd->kgts', query_here, key_here, preferred_element_type...  48.9 us
    another operation x1, loops' own time, shards(): lax.fori_loop(0, step_count, one_step, initial)  45.3 us
    dot_general x64, matrix products, softmax_update(): jnp.einsum('kgts,skd->kgtd', weights.astype(jnp.bfloat16), value_here, pr...  39.5 us
    reduce_sum x64, other arithmetic, softmax_update(): row_mass = row_mass * rescale + jnp.sum(weights, axis=3)  37.9 us
    all_gather x1, waiting for transfers between devices, shards(): gathered = lax.all_gather(projected[:, query_cols:], SP, axis=0, tiled=True)  35 us
    reshape x32, local copies, waits for them, and re-layouts, one_step(): block_rows[:, key_cols:2 * key_cols].reshape(step_rows, kv_heads_here, HEAD)  31.8 us
    all_to_all x1, blocking collectives, sum_at_owner(): lax.all_to_all(pieces, axis, split_axis=0, concat_axis=0, tiled=True)  19.5 us
  transfers between devices with their start and end apart: 2, of which 2 were waited for; matrix products, arithmetic and copies ran while one was open for 1% of the time, Pallas kernels for 0%

commit v1 on v0

--- a/solution.py
+++ b/solution.py
@@ -131,7 +131,9 @@
         jnp.zeros((2, kv_heads_here, group_size, half_rows), jnp.float32),
         jnp.zeros((2, kv_heads_here, group_size, half_rows, HEAD), jnp.float32),
     )
-    gathered = lax.all_gather(projected[:, query_cols:], SP, axis=0, tiled=True)
+    gathered = jnp.concatenate(
+        lax.all_to_all(jnp.stack([projected[:, query_cols:]] * lax.axis_size(SP)), SP, 0, 0), axis=0
+    )
     row_count = gathered.shape[0]
     piece_blocks = row_count // half_rows
     per_step = math.gcd(piece_blocks, max(1, 1024 // half_rows))

time: 390 us -> 633 us (1.62)
  blocking collectives: 68.7 us -> 312 us
  waiting for transfers between devices: 48.4 us -> 13.4 us
  local copies, waits for them, and re-layouts: 59.3 us -> 93.1 us
  between operations: 13.7 us -> 0.31 us
  starting transfers between devices: 4.29 us -> 16 us
    all_gather x2, blocking collectives: 49.1 us -> 294 us  [all_blocks(): pieces = lax.all_gather(pieces, axes[k])]
    all_gather x1 -> x0, waiting for transfers between devices: 35 us -> none  [shards(): gathered = lax.all_gather(projected[:, query_cols:], SP, axis=0, tiled=True)]
    unnamed x16 -> x20, local copies, waits for them, and re-layouts: 1.84 us -> 23.1 us
    all_to_all x0 -> x1, starting transfers between devices: none -> 11.6 us  [shards(): lax.all_to_all(jnp.stack([projected[:, query_cols:]] * lax.axis_size(SP))...]
    all_to_all x0 -> x1, local copies, waits for them, and re-layouts: none -> 9.04 us  [shards(): lax.all_to_all(jnp.stack([projected[:, query_cols:]] * lax.axis_size(SP))...]
  transfers between devices with their start and end apart: 2 -> 2, of which waited for: 2 -> 1; matrix products, arithmetic and copies ran while one was open for 1% -> 1% of each run, Pallas kernels for 0% -> 0%
where the time goes in v1:
time: 633 us; the launch traced here: 629 us
  blocking collectives  312 us (49%)
  local copies, waits for them, and re-layouts  93.1 us (15%)
  matrix products  91.5 us (14%)
  other arithmetic  55.4 us (9%)
  loops' own time  47.5 us (8%)
  starting transfers between devices  16 us (3%)
  waiting for transfers between devices  13.4 us (2%)
    all_gather x2, blocking collectives, all_blocks(): pieces = lax.all_gather(pieces, axes[k])  294 us
    dot_general x64, matrix products, softmax_update(): jnp.einsum('kgtd,skd->kgts', query_here, key_here, preferred_element_type...  49 us
    another operation x1, loops' own time, shards(): lax.fori_loop(0, step_count, one_step, initial)  45.4 us
    dot_general x64, matrix products, softmax_update(): jnp.einsum('kgts,skd->kgtd', weights.astype(jnp.bfloat16), value_here, pr...  39.5 us
    reduce_sum x64, other arithmetic, softmax_update(): row_mass = row_mass * rescale + jnp.sum(weights, axis=3)  37.9 us
    reshape x32, local copies, waits for them, and re-layouts, one_step(): block_rows[:, key_cols:2 * key_cols].reshape(step_rows, kv_heads_here, HEAD)  31.8 us
    unnamed x20, local copies, waits for them, and re-layouts  23.1 us
    dynamic_slice x32, local copies, waits for them, and re-layouts, one_step(): first_id = earliest[step_index]  18.8 us
  transfers between devices with their start and end apart: 2, of which 1 were waited for; matrix products, arithmetic and copies ran while one was open for 1% of the time, Pallas kernels for 0%

profile of v1, /device:TPU:504, one launch (start us, length us, event | category | flops | bytes accessed | tf_op | source)
XLA Modules:
  0.0 629.2 jit_solution(6939087339371117873)
XLA Ops:
  2.2 4.4 all-to-all-start
  8.3 13.4 %all-to-all-done = bf16[4,64,2048]{2,1,0:T(8,128)(2,1)S(1)} async-done(((bf16[4,64,2048]{2,1,0:T(8,128)(2,1)}), bf16[4,64,2048]{2,1,0:T(8,128)(2,1)S(1)}, u32[]{:S(2)}, u32[]{:S(2)}) %all-to-all-start) | async-done | bytes 1048608 | tf_op jit(solution)/shard_map/all_to_all | solution.py:16
  21.7 2.5 fusion.47
  24.3 4.0 stack.92
  28.3 11.6 %all-to-all-start.1 = ((bf16[128,256,132]{1,2,0:T(8,128)(2,1)}), bf16[128,256,132]{1,2,0:T(8,128)(2,1)}, u32[]{:S(2)}, u32[]{:S(2)}) async-start(bf16[128,256,132]{1,2,0:T(8,128)(2,1)} %stack.92), calls=%async_computation.1 | async-start | bytes 17825792 | tf_op jit(solution)/shard_map/all_to_all | solution.py:135
  40.5 291.7 %all-gather.2 = f32[64,2,4]{2,1,0:T(2,128)S(1)} all-gather(f32[1,2,4]{2,1,0:T(2,128)S(1)} %bitcast.224), channel_id=2, replica_groups=mesh['sp_0'=8,'sp_1'=8,'sp_2'=2,'tp'=4] {'sp_0','sp_1'}, dimensions={0}, use_global_device_ids=true | all-gather | bytes 2080 | tf_op jit(solution)/shard_map/all_gather | solution.py:33
  338.0 9.0 %copy.110 = bf16[128,256,132]{1,0,2:T(8,128)(2,1)} copy(bf16[128,256,132]{1,2,0:T(8,128)(2,1)} %all-to-all-done.1) | data formatting | bytes 17301504 | tf_op jit(solution)/shard_map/all_to_all | solution.py:135
  347.0 8.1 %pad.11 = bf16[136,128,256]{2,1,0:T(8,128)(2,1)} pad(bf16[132,128,256]{2,1,0:T(8,128)(2,1)} %bitcast.203, bf16[]{:T(256)} %constant.166.clone.1), padding=0_4x0_0x0_0 | pad | bytes 17563650
  355.1 13.1 %copy.100 = bf16[17,8,128,256]{3,1,2,0:T(8,128)(2,1)} copy(bf16[17,8,128,256]{3,2,1,0:T(8,128)(2,1)} %bitcast.202) | data formatting | bytes 17825792
  371.3 238.2 %while.18 = (s32[]{:T(128)}, f32[2,1,4,128]{3,2,1,0:T(4,128)S(1)}, f32[2,1,4,128]{3,2,1,0:T(4,128)S(1)}, f32[2,1,4,128,64]{3,4,2,1,0:T(8,128)S(1)}, s32[32]{0:T(...) while((s32[]{:T(128)}, f32[2,1,4,128]{3,2,1,0:T(4,128)S(1)}, ...), condition=%wide.region_16.17_spmd.clone, body=%wide.region_7.16_spmd.clone.sunk | while | flops 280433920 | bytes 16568895 | solution.py:192
  381.3 2.2 conditional.7
  388.7 2.2 conditional.7
  396.2 2.2 conditional.7
  403.6 2.2 conditional.7
  411.1 2.2 conditional.7
  418.5 2.2 conditional.7
  425.9 2.2 conditional.7
  433.4 2.2 conditional.7
  440.8 2.2 conditional.7
  448.2 2.2 conditional.7
  455.7 2.2 conditional.7
  463.1 2.2 conditional.7
  470.5 2.2 conditional.7
  478.0 2.2 conditional.7
  485.4 2.2 conditional.7
  492.8 2.2 conditional.7
  500.3 2.2 conditional.7
  507.7 2.2 conditional.7
  515.2 2.2 conditional.7
  589.5 2.2 conditional.7
  604.4 2.2 conditional.7
  610.1 18.1 %all_to_all.15 = bf16[4,64,2048]{2,1,0:T(8,128)(2,1)S(1)} all-to-all(bf16[4,64,2048]{2,1,0:T(8,128)(2,1)S(1)} %bitcast.208), channel_id=1, replica_groups=mesh['sp_0'=8,'sp_1'=8,'sp_2'=2,'tp'=4] {'tp'}, dimensions={0} | all-to-all | bytes 2097152 | tf_op jit(solution)/shard_map/all_to_all | solution.py:52
  (913 shorter events, 299.0 us)
Async XLA Ops:
  0.0 609.7 %copy-start = (bf16[256,2048]{1,0:T(8,128)(2,1)S(1)}, bf16[256,2048]{1,0:T(8,128)(2,1)}, u32[]{:S(2)}) copy-start(bf16[256,2048]{1,0:T(8,128)(2,1)} %param.19) | copy-start | bytes 3145732
  0.0 6.6 %copy-start.2 = (bf16[2048,64]{0,1:T(8,128)(2,1)S(1)}, bf16[2048,64]{0,1:T(8,128)(2,1)}, u32[]{:S(2)}) copy-start(bf16[2048,64]{0,1:T(8,128)(2,1)} %param.15) | copy-start | bytes 786436
  0.0 6.9 %copy-start.3 = (bf16[2048,64]{0,1:T(8,128)(2,1)S(1)}, bf16[2048,64]{0,1:T(8,128)(2,1)}, u32[]{:S(2)}) copy-start(bf16[2048,64]{0,1:T(8,128)(2,1)} %param.16) | copy-start | bytes 786436
  2.2 5.0 copy-start.4
  2.2 19.5 %all-to-all-start = ((bf16[4,64,2048]{2,1,0:T(8,128)(2,1)}), bf16[4,64,2048]{2,1,0:T(8,128)(2,1)S(1)}, u32[]{:S(2)}, u32[]{:S(2)}) async-start(bf16[4,64,2048]{2,1,0:T(8,128)(2,1)} %broadcast_in_dim.67), calls=%async_computation | async-start | bytes 2097152 | tf_op jit(solution)/shard_map/all_to_all | solution.py:16
  24.2 15.9 %copy-start.1 = (bf16[256,388]{0,1:T(8,128)(2,1)}, bf16[256,388]{0,1:T(8,128)(2,1)S(1)}, u32[]{:S(2)}) copy-start(bf16[256,388]{0,1:T(8,128)(2,1)S(1)} %fusion.47) | copy-start | bytes 595972
  28.3 11.9 %copy-start.5 = (f32[4]{0:T(128)S(1)}, f32[4]{0:T(128)}, u32[]{:S(2)}) copy-start(f32[4]{0:T(128)} %param.18) | copy-start | bytes 52
  28.3 309.7 %all-to-all-start.1 = ((bf16[128,256,132]{1,2,0:T(8,128)(2,1)}), bf16[128,256,132]{1,2,0:T(8,128)(2,1)}, u32[]{:S(2)}, u32[]{:S(2)}) async-start(bf16[128,256,132]{1,2,0:T(8,128)(2,1)} %stack.92), calls=%async_computation.1 | async-start | bytes 17825792 | tf_op jit(solution)/shard_map/all_to_all | solution.py:135
  40.3 297.6 %slice-start = ((bf16[256,388]{0,1:T(8,128)(2,1)}), bf16[256,256]{0,1:T(8,128)(2,1)S(1)}, s32[]{:S(2)}) async-start(bf16[256,388]{0,1:T(8,128)(2,1)} %copy-done.1), calls=%async_computation.3 | async-start | bytes 262144 | tf_op jit(solution)/shard_map/slice | solution.py:109
